TPU v7x, 32 devices: a whole 2x2x4 slice. The times are simulated.
32 devices in a mesh: grp: 2 (over y), fs: 4 (over z), tp: 4 (over x, core).
Axes of the slice: x: 2, y: 2, z: 4, core: 2. Of those that a mesh axis runs over, the one named last changes fastest.
Arguments:
- tokens: bfloat16 [4096, 2048], P(('grp', 'fs')), parts along dimension 0, may hold values from -6 to 6
- pre_gain: float32 [2048], replicated, may hold values from 0.1 to 1.9
- up_weight: float32 [2048, 8192], P('fs', 'tp'), may hold values from -0.125 to 0.125
- up_scale: float32 [8192], P('tp'), may hold values from 0.3 to 3
- down_weight: float32 [8192, 2048], P('tp', 'fs'), may hold values from -0.0625 to 0.0625
- down_scale: float32 [2048], P('fs'), may hold values from 0.3 to 3
- post_gain: float32 [2048], replicated, may hold values from 0.1 to 1.9
Outputs:
- mixed: bfloat16 [4096, 2048], P(('grp', 'fs')), parts along dimension 0
There are 2 independent parts, one for each index of `grp`. A program takes and returns all parts, laid end to end along the dimension named above; an argument that names none is the same for every part. Nothing has to cross between parts.
All inputs are finite; a program needn't handle non-finite values.
Results may differ from a plain program's by a relative error of at most 0.01.
Values may be sent and summed in bfloat16 or wider, within the bound.
A program may use at most 64 MiB of HBM per device.

v0:
```python
import jax
import jax.numpy as jnp
from jax import lax
from jax.sharding import PartitionSpec as P

epsilon = 1e-06


def rms_rows(values, scaling):
    return values * lax.rsqrt(jnp.mean(values * values, axis=-1, keepdims=True) + epsilon) * scaling


def activate(lifted, up_scale):
    return jnp.square(jax.nn.relu(lifted * up_scale)).astype(jnp.bfloat16)


def on_device(tokens, pre_gain, up_weight, up_scale, down_weight, down_scale, post_gain):
    residual = tokens.astype(jnp.float32)
    normed = rms_rows(residual, pre_gain).astype(jnp.bfloat16)
    up_cast = up_weight.astype(jnp.bfloat16)
    down_cast = down_weight.astype(jnp.bfloat16)
    column_scales = lax.all_gather(down_scale, "fs", axis=0, tiled=True)
    up_full, down_full = (
        lax.all_gather(up_cast, "fs", axis=0, tiled=True),
        lax.all_gather(down_cast, "fs", axis=1, tiled=True),
    )
    lifted = jnp.dot(normed, up_full, preferred_element_type=jnp.float32)
    hidden = activate(lifted, up_scale)
    partials = jnp.dot(hidden, down_full, preferred_element_type=jnp.float32)
    partials = (partials * column_scales).astype(jnp.bfloat16)
    summed = lax.psum(partials, "tp").astype(jnp.float32)
    branch = lax.optimization_barrier(summed.astype(jnp.bfloat16)).astype(jnp.float32)
    return (residual + rms_rows(branch, post_gain)).astype(jnp.bfloat16)


def solution(mesh):
    placed = (P(("grp", "fs"), None), P(), P("fs", "tp"), P("tp"), P("tp", "fs"), P("fs"), P())
    return jax.shard_map(
        on_device, mesh=mesh, in_specs=placed, out_specs=P(("grp", "fs"), None), check_vma=False
    )
```

profile of v0, /device:TPU:0, one launch (start us, length us, event | category | flops | bytes accessed | tf_op | source)
XLA Modules:
  0.0 390.7 jit_solution(1393398002839084678)
XLA Ops:
  6.5 0.0 all-gather.4.cloned.1.call-start
  6.5 3.8 convert_element_type.28
  10.4 0.0 all-gather.4.cloned.1.call-update
  10.4 0.0 copy-start.2
  10.4 0.0 copy-start
  10.4 0.0 copy-start.3
  10.4 0.0 copy-start.4
  10.5 0.0 all-gather.6.cloned.1.call-start
  10.5 3.9 %convert_element_type.30 = bf16[2048,512]{1,0:T(8,128)(2,1)} convert(f32[2048,512]{1,0:T(8,128)} %param.11) | non-fusion elementwise | flops 1048576 | bytes 6291456 | tf_op jit(solution)/shard_map/convert_element_type | solution.py:21
  14.4 0.0 all-gather.6.cloned.1.call-update
  14.4 0.0 all-reduce.2.cloned.1.call-start
  14.5 0.0 copy-done.2
  14.5 13.7 %all-gather = f32[4,1,512]{2,1,0:T(1,128)S(1)} all-gather(f32[1,1,512]{2,1,0:T(1,128)S(1)} %bitcast.10), channel_id=1, replica_groups=mesh['grp'=2,'fs'=4,'tp'=4] {'fs'}, dimensions={0}, use_global_device_ids=true | all-gather | bytes 10240 | tf_op jit(solution)/shard_map/all_gather | solution.py:22
  28.2 0.0 copy-done
  28.2 0.5 fusion.2
  28.7 134.2 %all-gather.4.cloned.1.call-done = bf16[2048,2048]{1,0:T(8,128)(2,1)} async-done(((bf16[512,2048]{1,0:T(8,128)(2,1)}), bf16[2048,2048]{1,0:T(8,128)(2,1)}) %all-gather.4.cloned.1.call-update) | async-done | bytes 8388624 | tf_op jit(solution)/shard_map/all_gather | solution.py:24
  162.9 149.4 %all-gather.6.cloned.1.call-done = bf16[2048,2048]{1,0:T(8,128)(2,1)} async-done(((bf16[2048,512]{1,0:T(8,128)(2,1)}), bf16[2048,2048]{1,0:T(8,128)(2,1)}) %all-gather.6.cloned.1.call-update) | async-done | bytes 8388624 | tf_op jit(solution)/shard_map/all_gather | solution.py:25
  312.3 0.0 copy-done.3
  312.3 0.0 copy-done.4
  312.3 16.0 %multiply_convert_fusion = bf16[512,2048]{1,0:T(8,128)(2,1)} fusion(bf16[2048,2048]{1,0:T(8,128)(2,1)} %all-gather.6.cloned.1.call-done, f32[2048]{0:T(1024)S(1)} %bitcast.9, bf16[2048,2048]{1,0:T(8,128)(2,1)} %all-gather.4.cloned.1.call-done, bf16[512,2048]{1,0:T(8,128)(2,1)S(1)} %copy-done, f32[2048]{0:T(1024)S(1)} %copy-done.3, f32[2048]{0:T(1024)S(1)} %copy-done.4, ...), kind=kOutput, calls=%fused_computation.11 | convolution fusion | flops 8600420352 | bytes 20998144 | tf_op jit(solution)/shard_map/dot_general | solution.py:29
  328.3 0.0 copy-start.1
  328.3 0.0 all-reduce.2.cloned.1.call-update
  328.3 49.7 %all-reduce.2.cloned.1.call-done = bf16[512,2048]{1,0:T(8,128)(2,1)} async-done(((bf16[512,2048]{1,0:T(8,128)(2,1)}), bf16[512,2048]{1,0:T(8,128)(2,1)}) %all-reduce.2.cloned.1.call-update) | async-done | bytes 2097168 | tf_op jit(solution)/shard_map/psum | solution.py:31
  378.0 2.1 fusion
  380.1 0.0 copy-done.1
  380.1 4.1 %fusion.5 = bf16[512,2048]{1,0:T(8,128)(2,1)} fusion(bf16[512,2048]{1,0:T(8,128)(2,1)} %all-reduce.2.cloned.1.call-done, bf16[512,2048]{1,0:T(8,128)(2,1)S(1)} %copy-done, f32[2048]{0:T(1024)S(1)} %copy-done.1, f32[512]{0:T(512)S(1)} %add_rsqrt_fusion), kind=kLoop, calls=%fused_computation.10 | loop fusion | flops 6291456 | bytes 6301696 | tf_op jit(solution)/shard_map/convert_element_type | solution.py:33
  (2 shorter events, 0.0 us)
Async XLA Ops:
  6.5 156.4 %all-gather.4.cloned.1.call-start = ((), (), s32[]{:S(2)}) async-start(), calls=%async_computation | async-start | bytes 10485760 | tf_op jit(solution)/shard_map/all_gather | solution.py:24
  10.4 4.1 %copy-start.2 = (f32[512]{0:T(512)S(1)}, f32[512]{0:T(512)}, u32[]{:S(2)}) copy-start(f32[512]{0:T(512)} %param.12) | copy-start | bytes 6148
  10.4 17.8 %copy-start = (bf16[512,2048]{1,0:T(8,128)(2,1)S(1)}, bf16[512,2048]{1,0:T(8,128)(2,1)}, u32[]{:S(2)}) copy-start(bf16[512,2048]{1,0:T(8,128)(2,1)} %param.7) | copy-start | bytes 6291460
  10.4 301.9 %copy-start.3 = (f32[2048]{0:T(1024)S(1)}, f32[2048]{0:T(1024)}, u32[]{:S(2)}) copy-start(f32[2048]{0:T(1024)} %param.10) | copy-start | bytes 24580
  10.4 301.9 %copy-start.4 = (f32[2048]{0:T(1024)S(1)}, f32[2048]{0:T(1024)}, u32[]{:S(2)}) copy-start(f32[2048]{0:T(1024)} %param.8) | copy-start | bytes 24580
  10.5 301.9 %all-gather.6.cloned.1.call-start = ((), (), s32[]{:S(2)}) async-start(), calls=%async_computation.1 | async-start | bytes 10485760 | tf_op jit(solution)/shard_map/all_gather | solution.py:25
  14.4 363.6 %all-reduce.2.cloned.1.call-start = ((), (), s32[]{:S(2)}) async-start(), calls=%async_computation.2 | async-start | bytes 4194304 | tf_op jit(solution)/shard_map/psum | solution.py:31
  328.3 51.8 %copy-start.1 = (f32[2048]{0:T(1024)S(1)}, f32[2048]{0:T(1024)}, u32[]{:S(2)}) copy-start(f32[2048]{0:T(1024)} %param.13) | copy-start | bytes 24580
Sparse Core Ops, SparseCore 0:
  10.5 152.3 all-gather.3
  164.5 147.7 all-gather.5
  328.4 49.5 all-reduce.1
where the time goes:
time: 391 us
  waiting for transfers between devices  333 us (85%)
  matrix products  16 us (4%)
  other arithmetic  14.4 us (4%)
  blocking collectives  13.7 us (4%)
  between operations  13.2 us (3%)
    all_gather x1, waiting for transfers between devices, on_device(): lax.all_gather(down_cast, 'fs', axis=1, tiled=True)  149 us
    all_gather x1, waiting for transfers between devices, on_device(): lax.all_gather(up_cast, 'fs', axis=0, tiled=True)  134 us
    psum x1, waiting for transfers between devices, on_device(): summed = lax.psum(partials, 'tp').astype(jnp.float32)  49.7 us
    dot_general x1, matrix products, on_device(): partials = jnp.dot(hidden, down_full, preferred_element_type=jnp.float32)  16 us
    all_gather x1, blocking collectives, on_device(): column_scales = lax.all_gather(down_scale, 'fs', axis=0, tiled=True)  13.7 us
  transfers between devices with their start and end apart: 3, of which 3 were waited for; matrix products, arithmetic and copies ran while one was open for 1% of the time, Pallas kernels for 0%

commit v1 on v0

--- a/solution.py
+++ b/solution.py
@@ -21,7 +21,9 @@
     down_cast = down_weight.astype(jnp.bfloat16)
     column_scales = lax.all_gather(down_scale, "fs", axis=0, tiled=True)
     up_full, down_full = (
-        lax.all_gather(up_cast, "fs", axis=0, tiled=True),
+        jnp.concatenate(
+            lax.all_to_all(jnp.stack([up_cast] * lax.axis_size("fs")), "fs", 0, 0), axis=0
+        ),
         lax.all_gather(down_cast, "fs", axis=1, tiled=True),
     )
     lifted = jnp.dot(normed, up_full, preferred_element_type=jnp.float32)

time: 391 us -> 424 us (1.084)
  blocking collectives: 13.7 us -> 320 us
  waiting for transfers between devices: 333 us -> 50 us
  starting transfers between devices: 0.09 us -> 6.43 us
  local copies, waits for them, and re-layouts: 0.03 us -> 4.33 us
    all_gather x1, blocking collectives: 13.7 us -> 320 us  [on_device(): column_scales = lax.all_gather(down_scale, 'fs', axis=0, tiled=True)]
    all_gather x1, waiting for transfers between devices: 149 us -> 0.02 us  [on_device(): lax.all_gather(down_cast, 'fs', axis=1, tiled=True)]
    all_gather x1 -> x0, waiting for transfers between devices: 134 us -> none  [on_device(): lax.all_gather(up_cast, 'fs', axis=0, tiled=True)]
    all_to_all x0 -> x1, starting transfers between devices: none -> 6.35 us  [on_device(): lax.all_to_all(jnp.stack([up_cast] * lax.axis_size('fs')), 'fs', 0, 0)]
    another operation x0 -> x1, local copies, waits for them, and re-layouts: none -> 4.31 us  [on_device(): jnp.stack([up_cast] * lax.axis_size('fs'))]
  transfers between devices with their start and end apart: 3 -> 3, of which waited for: 3 -> 1; matrix products, arithmetic and copies ran while one was open for 1% -> 1% of each run, Pallas kernels for 0% -> 0%
where the time goes in v1:
time: 424 us; the launch traced here: 423 us
  blocking collectives  320 us (75%)
  waiting for transfers between devices  50 us (12%)
  matrix products  16 us (4%)
  between operations  13.5 us (3%)
  other arithmetic  13.1 us (3%)
  starting transfers between devices  6.43 us (2%)
  local copies, waits for them, and re-layouts  4.33 us (1%)
    all_gather x1, blocking collectives, on_device(): column_scales = lax.all_gather(down_scale, 'fs', axis=0, tiled=True)  320 us
    psum x1, waiting for transfers between devices, on_device(): summed = lax.psum(partials, 'tp').astype(jnp.float32)  49.9 us
    dot_general x1, matrix products, on_device(): partials = jnp.dot(hidden, down_full, preferred_element_type=jnp.float32)  16 us
  transfers between devices with their start and end apart: 3, of which 1 were waited for; matrix products, arithmetic and copies ran while one was open for 1% of the time, Pallas kernels for 0%

profile of v1, /device:TPU:0, one launch (start us, length us, event | category | flops | bytes accessed | tf_op | source)
XLA Modules:
  0.0 423.3 jit_solution(11032540553369062330)
XLA Ops:
  6.5 2.5 convert_element_type.28
  9.0 4.3 %stack.2 = bf16[4,512,2048]{2,1,0:T(8,128)(2,1)} broadcast(bf16[512,2048]{1,0:T(8,128)(2,1)S(1)} %convert_element_type.28), dimensions={1,2} | broadcast | bytes 10485760 | tf_op jit(solution)/shard_map/stack | solution.py:25
  13.3 6.3 %all-to-all-start = ((bf16[4,512,2048]{2,1,0:T(8,128)(2,1)}), bf16[4,512,2048]{2,1,0:T(8,128)(2,1)}, u32[]{:S(2)}, u32[]{:S(2)}) async-start(bf16[4,512,2048]{2,1,0:T(8,128)(2,1)} %stack.2), calls=%async_computation | async-start | bytes 16777216 | tf_op jit(solution)/shard_map/all_to_all | solution.py:25
  19.7 0.0 copy-start.2
  19.7 0.0 copy-start
  19.7 0.0 copy-start.3
  19.7 0.0 copy-start.4
  19.7 0.0 all-gather.3.cloned.1.call-start
  19.8 3.9 convert_element_type.30
  23.7 0.0 all-gather.3.cloned.1.call-update
  23.7 0.0 all-reduce.2.cloned.1.call-start
  23.8 0.0 copy-done.2
  23.8 320.0 %all-gather = f32[4,1,512]{2,1,0:T(1,128)S(1)} all-gather(f32[1,1,512]{2,1,0:T(1,128)S(1)} %bitcast.11), channel_id=1, replica_groups=mesh['grp'=2,'fs'=4,'tp'=4] {'fs'}, dimensions={0}, use_global_device_ids=true | all-gather | bytes 10240 | tf_op jit(solution)/shard_map/all_gather | solution.py:22
  343.8 0.0 copy-done
  343.8 0.5 fusion.2
  344.3 0.0 all-to-all-done
  344.3 0.0 all-gather.3.cloned.1.call-done
  344.3 0.0 copy-done.3
  344.3 0.0 copy-done.4
  344.3 16.0 %multiply_convert_fusion = bf16[512,2048]{1,0:T(8,128)(2,1)} fusion(bf16[2048,2048]{1,0:T(8,128)(2,1)} %all-gather.3.cloned.1.call-done, f32[2048]{0:T(1024)S(1)} %bitcast.10, bf16[2048,2048]{1,0:T(8,128)(2,1)} %bitcast, bf16[512,2048]{1,0:T(8,128)(2,1)S(1)} %copy-done, f32[2048]{0:T(1024)S(1)} %copy-done.3, f32[2048]{0:T(1024)S(1)} %copy-done.4, ...), kind=kOutput, calls=%fused_computation.11 | convolution fusion | flops 8600420352 | bytes 20998144 | tf_op jit(solution)/shard_map/dot_general | solution.py:31
  360.3 0.0 copy-start.1
  360.3 0.0 all-reduce.2.cloned.1.call-update
  360.3 49.9 %all-reduce.2.cloned.1.call-done = bf16[512,2048]{1,0:T(8,128)(2,1)} async-done(((bf16[512,2048]{1,0:T(8,128)(2,1)}), bf16[512,2048]{1,0:T(8,128)(2,1)}) %all-reduce.2.cloned.1.call-update) | async-done | bytes 2097168 | tf_op jit(solution)/shard_map/psum | solution.py:33
  410.3 2.1 fusion
  412.3 0.0 copy-done.1
  412.3 4.1 fusion.5
  (2 shorter events, 0.0 us)
Async XLA Ops:
  13.3 330.9 %all-to-all-start = ((bf16[4,512,2048]{2,1,0:T(8,128)(2,1)}), bf16[4,512,2048]{2,1,0:T(8,128)(2,1)}, u32[]{:S(2)}, u32[]{:S(2)}) async-start(bf16[4,512,2048]{2,1,0:T(8,128)(2,1)} %stack.2), calls=%async_computation | async-start | bytes 16777216 | tf_op jit(solution)/shard_map/all_to_all | solution.py:25
  19.7 4.1 copy-start.2
  19.7 324.1 %copy-start = (bf16[512,2048]{1,0:T(8,128)(2,1)S(1)}, bf16[512,2048]{1,0:T(8,128)(2,1)}, u32[]{:S(2)}) copy-start(bf16[512,2048]{1,0:T(8,128)(2,1)} %param.7) | copy-start | bytes 6291460
  19.7 324.6 %copy-start.3 = (f32[2048]{0:T(1024)S(1)}, f32[2048]{0:T(1024)}, u32[]{:S(2)}) copy-start(f32[2048]{0:T(1024)} %param.10) | copy-start | bytes 24580
  19.7 324.6 %copy-start.4 = (f32[2048]{0:T(1024)S(1)}, f32[2048]{0:T(1024)}, u32[]{:S(2)}) copy-start(f32[2048]{0:T(1024)} %param.8) | copy-start | bytes 24580
  19.7 324.6 %all-gather.3.cloned.1.call-start = ((), (), s32[]{:S(2)}) async-start(), calls=%async_computation.1 | async-start | bytes 10485760 | tf_op jit(solution)/shard_map/all_gather | solution.py:27
  23.7 386.6 %all-reduce.2.cloned.1.call-start = ((), (), s32[]{:S(2)}) async-start(), calls=%async_computation.2 | async-start | bytes 4194304 | tf_op jit(solution)/shard_map/psum | solution.py:33
  360.3 52.0 %copy-start.1 = (f32[2048]{0:T(1024)S(1)}, f32[2048]{0:T(1024)}, u32[]{:S(2)}) copy-start(f32[2048]{0:T(1024)} %param.13) | copy-start | bytes 24580
Sparse Core Ops, SparseCore 0:
  23.8 293.6 all-gather.2
  360.5 49.7 all-reduce.1
